TPU v7x, 32 devices: a whole 2x2x4 slice. The times are simulated.
32 devices in a mesh: fs: 16 (over z, y, x), tp: 2 (over core).
Axes of the slice: x: 2, y: 2, z: 4, core: 2. Of those that a mesh axis runs over, the one named last changes fastest.
Arguments:
- tokens: bfloat16 [8192, 2048], P('fs', 'tp'), may hold values from -24 to 24
- u_weight: bfloat16 [2048, 1024], P('fs', 'tp'), may hold values from -0.125 to 0.125
- v_weight: bfloat16 [2048, 1024], P('fs', 'tp'), may hold values from -0.125 to 0.125
- sg_gain: float32 [1024], P('tp'), may hold values from 0.1 to 1.9
- spatial_weight: bfloat16 [8, 128, 128], P('tp'), may hold values from -0.5 to 0.5
- spatial_bias: float32 [8, 128], P('tp'), may hold values from 0.1 to 1.9
- out_weight: bfloat16 [1024, 2048], P('tp', 'fs'), may hold values from -0.1875 to 0.1875
- gain_one: float32 [2048], P('tp'), may hold values from 0.1 to 1.9
- gate_weight: bfloat16 [2048, 5632], P('fs', 'tp'), may hold values from -0.125 to 0.125
- up_weight: bfloat16 [2048, 5632], P('fs', 'tp'), may hold values from -0.125 to 0.125
- down_weight: bfloat16 [5632, 2048], P('tp', 'fs'), may hold values from -0.078125 to 0.078125
- gain_two: float32 [2048], P('tp'), may hold values from 0.1 to 1.9
Outputs:
- layer_out: bfloat16 [8192, 2048], P('fs', 'tp')
All inputs are finite; a program needn't handle non-finite values.
Results may differ from a plain program's by a relative error of at most 0.014.
Values may be sent and summed in bfloat16 or wider, within the bound.
A program may use at most 128 MiB of HBM per device.

v0:
```python
import jax
import jax.numpy as jnp
from jax import lax
from jax.sharding import PartitionSpec as P

EPS = 1e-05
ALPHA = 2.0**0.25


def add_rows(left, piece):
    return jnp.dot(left, piece, preferred_element_type=jnp.float32)


def scaled_rows(vals, sums, gain, count):
    mean = sums[0][:, None] / count
    square = sums[1][:, None] / count
    return (vals - mean) * lax.rsqrt(square - mean * mean + EPS) * gain[None, :]


def on_device(
    tokens,
    u_weight,
    v_weight,
    sg_gain,
    spatial_weight,
    spatial_bias,
    out_weight,
    gain_one,
    gate_weight,
    up_weight,
    down_weight,
    gain_two,
):
    parts = lax.axis_size("tp")
    whole = lax.all_gather(tokens, "tp", axis=1, tiled=True)
    rows = whole.shape[0]
    width_sg = u_weight.shape[1]

    def add_one(piece):
        return add_rows(whole, piece)

    pre_u = add_one(lax.all_gather(u_weight, "fs", axis=0, tiled=True))
    pre_v = add_one(lax.all_gather(v_weight, "fs", axis=0, tiled=True))
    gated = jax.nn.gelu(pre_u)
    valued = jax.nn.gelu(pre_v)
    stats = lax.psum((jnp.sum(valued, axis=1), jnp.sum(valued * valued, axis=1)), "tp")
    normed = scaled_rows(valued, stats, sg_gain, width_sg * parts).astype(jnp.bfloat16)
    groups_here = spatial_weight.shape[0]
    block = spatial_weight.shape[1]
    group_width = width_sg // groups_here
    shaped = normed.reshape(rows // block, block, groups_here, group_width)
    lower = jnp.tril(jnp.ones((block, block), jnp.bool_))
    masked = jnp.where(lower[None], spatial_weight, jnp.zeros_like(spatial_weight))
    mixed = jnp.einsum("gij,njgd->nigd", masked, shaped, preferred_element_type=jnp.float32)
    mixed = mixed + spatial_bias.T[None, :, :, None]
    gated_out = (gated * mixed.reshape(rows, width_sg)).astype(jnp.bfloat16)
    terms = jnp.dot(
        gated_out,
        lax.all_gather(out_weight, "fs", axis=1, tiled=True),
        preferred_element_type=jnp.float32,
    )
    mix = lax.psum_scatter(terms.astype(jnp.bfloat16), "tp", scatter_dimension=1, tiled=True)
    resid = ALPHA * tokens.astype(jnp.float32) + mix.astype(jnp.float32)
    first_sums = lax.psum((jnp.sum(resid, axis=1), jnp.sum(resid * resid, axis=1)), "tp")
    first = scaled_rows(resid, first_sums, gain_one, resid.shape[1] * parts).astype(jnp.bfloat16)
    whole_first = lax.all_gather(first, "tp", axis=1, tiled=True)

    def add_first(piece):
        return add_rows(whole_first, piece)

    gate = add_first(lax.all_gather(gate_weight, "fs", axis=0, tiled=True))
    upper = add_first(lax.all_gather(up_weight, "fs", axis=0, tiled=True))
    hidden = (jax.nn.silu(gate) * upper).astype(jnp.bfloat16)
    ffn_terms = jnp.dot(
        hidden,
        lax.all_gather(down_weight, "fs", axis=1, tiled=True),
        preferred_element_type=jnp.float32,
    )
    ffn = lax.psum_scatter(ffn_terms.astype(jnp.bfloat16), "tp", scatter_dimension=1, tiled=True)
    second = ALPHA * first.astype(jnp.float32) + ffn.astype(jnp.float32)
    last_sums = lax.psum((jnp.sum(second, axis=1), jnp.sum(second * second, axis=1)), "tp")
    return scaled_rows(second, last_sums, gain_two, second.shape[1] * parts).astype(jnp.bfloat16)


def solution(mesh):
    return jax.shard_map(
        on_device,
        mesh=mesh,
        in_specs=(
            P("fs", "tp"),
            P("fs", "tp"),
            P("fs", "tp"),
            P("tp"),
            P("tp", None, None),
            P("tp", None),
            P("tp", "fs"),
            P("tp"),
            P("fs", "tp"),
            P("fs", "tp"),
            P("tp", "fs"),
            P("tp"),
        ),
        out_specs=P("fs", "tp"),
        check_vma=False,
    )
```

profile of v0, /device:TPU:0, one launch (start us, length us, event | category | flops | bytes accessed | tf_op | source)
XLA Modules:
  0.0 759.9 jit_solution(2212430606449240204)
XLA Ops:
  6.5 0.7 all-gather.9.cloned.1.call-update
  9.4 12.8 %all-gather.9.cloned.1.call-done = bf16[512,2048]{1,0:T(8,128)(2,1)} async-done(((bf16[512,1024]{1,0:T(8,128)(2,1)}), bf16[512,2048]{1,0:T(8,128)(2,1)}) %all-gather.9.cloned.1.call-update) | async-done | bytes 2097168 | tf_op jit(solution)/shard_map/all_gather | solution.py:35
  22.2 64.4 %all-gather.13.cloned.1.call-done = bf16[2048,512]{1,0:T(8,128)(2,1)} async-done(((bf16[128,512]{1,0:T(8,128)(2,1)}), bf16[2048,512]{1,0:T(8,128)(2,1)}) %all-gather.13.cloned.1.call-update) | async-done | bytes 2097168 | tf_op jit(solution)/shard_map/all_gather | solution.py:43
  86.6 3.8 fusion.35
  90.4 2.6 all-reduce.2
  94.4 54.1 %all-gather.11.cloned.1.call-done = bf16[2048,512]{1,0:T(8,128)(2,1)} async-done(((bf16[128,512]{1,0:T(8,128)(2,1)}), bf16[2048,512]{1,0:T(8,128)(2,1)}) %all-gather.11.cloned.1.call-update) | async-done | bytes 2097168 | tf_op jit(solution)/shard_map/all_gather | solution.py:42
  148.5 64.3 %all-gather.15.cloned.1.call-done = bf16[512,2048]{1,0:T(8,128)(2,1)} async-done(((bf16[512,128]{1,0:T(8,128)(2,1)}), bf16[512,2048]{1,0:T(8,128)(2,1)}) %all-gather.15.cloned.1.call-update) | async-done | bytes 2097168 | tf_op jit(solution)/shard_map/all_gather | solution.py:59
  212.9 6.8 convolution_convert_fusion.1
  219.7 7.9 %reduce-scatter.3.cloned.1.call-done = bf16[512,1024]{1,0:T(8,128)(2,1)} async-done(((bf16[512,2048]{1,0:T(8,128)(2,1)}), bf16[512,1024]{1,0:T(8,128)(2,1)}) %reduce-scatter.3.cloned.1.call-update) | async-done | bytes 1048592 | tf_op jit(solution)/shard_map/reduce_scatter | solution.py:62
  227.6 1.9 fusion
  229.5 2.5 all-reduce.1
  232.0 1.5 multiply_convert_fusion.2
  233.6 0.7 all-gather.19.cloned.1.call-update
  234.4 0.7 all-gather.21.cloned.1.call-update
  236.1 9.5 %all-gather.17.cloned.1.call-done = bf16[512,2048]{1,0:T(8,128)(2,1)} async-done(((bf16[512,1024]{1,0:T(8,128)(2,1)}), bf16[512,2048]{1,0:T(8,128)(2,1)}) %all-gather.17.cloned.1.call-update) | async-done | bytes 2097168 | tf_op jit(solution)/shard_map/all_gather | solution.py:66
  245.6 145.4 %all-gather.19.cloned.1.call-done = bf16[2048,2816]{1,0:T(8,128)(2,1)} async-done(((bf16[128,2816]{1,0:T(8,128)(2,1)}), bf16[2048,2816]{1,0:T(8,128)(2,1)}) %all-gather.19.cloned.1.call-update) | async-done | bytes 11534352 | tf_op jit(solution)/shard_map/all_gather | solution.py:71
  391.0 12.5 %fusion.38 = f32[512,2816]{1,0:T(8,128)} fusion(bf16[512,2048]{1,0:T(8,128)(2,1)} %all-gather.17.cloned.1.call-done, bf16[2048,2816]{1,0:T(8,128)(2,1)} %all-gather.19.cloned.1.call-done), kind=kOutput, calls=%fused_computation.57 | convolution fusion | flops 5905580032 | bytes 19398656 | tf_op jit(solution)/shard_map/dot_general | solution.py:11
  403.5 129.9 %all-gather.21.cloned.1.call-done = bf16[2048,2816]{1,0:T(8,128)(2,1)} async-done(((bf16[128,2816]{1,0:T(8,128)(2,1)}), bf16[2048,2816]{1,0:T(8,128)(2,1)}) %all-gather.21.cloned.1.call-update) | async-done | bytes 11534352 | tf_op jit(solution)/shard_map/all_gather | solution.py:72
  533.4 183.0 %all-gather.23.cloned.1.call-done = bf16[2816,2048]{1,0:T(8,128)(2,1)} async-done(((bf16[2816,128]{1,0:T(8,128)(2,1)}), bf16[2816,2048]{1,0:T(8,128)(2,1)}) %all-gather.23.cloned.1.call-update) | async-done | bytes 11534352 | tf_op jit(solution)/shard_map/all_gather | solution.py:76
  716.4 22.8 %convolution_convert_fusion = bf16[512,2048]{1,0:T(8,128)(2,1)} fusion(bf16[2816,2048]{1,0:T(8,128)(2,1)} %all-gather.23.cloned.1.call-done, f32[512,2816]{1,0:T(8,128)} %fusion.38, bf16[512,2048]{1,0:T(8,128)(2,1)S(1)} %copy-done.9, bf16[2048,2816]{1,0:T(8,128)(2,1)} %all-gather.21.cloned.1.call-done), kind=kOutput, calls=%fused_computation.1 | convolution fusion | flops 11820859392 | bytes 33030144 | tf_op jit(solution)/shard_map/dot_general | solution.py:74
  739.2 8.0 %reduce-scatter.5.cloned.1.call-done = bf16[512,1024]{1,0:T(8,128)(2,1)} async-done(((bf16[512,2048]{1,0:T(8,128)(2,1)}), bf16[512,1024]{1,0:T(8,128)(2,1)}) %reduce-scatter.5.cloned.1.call-update) | async-done | bytes 1048592 | tf_op jit(solution)/shard_map/reduce_scatter | solution.py:79
  747.1 1.9 fusion.1
  749.0 2.5 all-reduce
  751.5 1.5 multiply_convert_fusion.1
  (45 shorter events, 4.6 us)
Async XLA Ops:
  6.5 15.7 %all-gather.9.cloned.1.call-start = ((), (), s32[]{:S(2)}) async-start(), calls=%async_computation.2 | async-start | bytes 3145728 | tf_op jit(solution)/shard_map/all_gather | solution.py:35
  7.3 79.3 %all-gather.13.cloned.1.call-start = ((), (), s32[]{:S(2)}) async-start(), calls=%async_computation.4 | async-start | bytes 2228224 | tf_op jit(solution)/shard_map/all_gather | solution.py:43
  8.0 140.5 %all-gather.11.cloned.1.call-start = ((), (), s32[]{:S(2)}) async-start(), calls=%async_computation.3 | async-start | bytes 2228224 | tf_op jit(solution)/shard_map/all_gather | solution.py:42
  8.7 204.1 %all-gather.15.cloned.1.call-start = ((), (), s32[]{:S(2)}) async-start(), calls=%async_computation.5 | async-start | bytes 2228224 | tf_op jit(solution)/shard_map/all_gather | solution.py:59
  9.3 218.3 %reduce-scatter.3.cloned.1.call-start = ((), (), s32[]{:S(2)}) async-start(), calls=%async_computation.6 | async-start | bytes 3145728 | tf_op jit(solution)/shard_map/reduce_scatter | solution.py:62
  9.4 83.7 %copy-start.7 = (f32[512]{0:T(512)S(1)}, f32[512]{0:T(512)}, u32[]{:S(2)}) copy-start(f32[512]{0:T(512)} %param.15) | copy-start | bytes 6148
  90.4 3.2 copy-start.4
  90.4 3.2 copy-start.8
  219.7 8.0 %copy-start.1 = (bf16[512,1024]{1,0:T(8,128)(2,1)S(1)}, bf16[512,1024]{1,0:T(8,128)(2,1)}, u32[]{:S(2)}) copy-start(bf16[512,1024]{1,0:T(8,128)(2,1)} %param.12) | copy-start | bytes 3145732
  219.7 12.4 %copy-start.5 = (f32[1024]{0:T(1024)S(1)}, f32[1024]{0:T(1024)}, u32[]{:S(2)}) copy-start(f32[1024]{0:T(1024)} %param.19) | copy-start | bytes 12292
  219.7 25.9 %all-gather.17.cloned.1.call-start = ((), (), s32[]{:S(2)}) async-start(), calls=%async_computation.7 | async-start | bytes 3145728 | tf_op jit(solution)/shard_map/all_gather | solution.py:66
  227.6 4.4 copy-start.2
  233.6 157.4 %all-gather.19.cloned.1.call-start = ((), (), s32[]{:S(2)}) async-start(), calls=%async_computation.8 | async-start | bytes 12255232 | tf_op jit(solution)/shard_map/all_gather | solution.py:71
  234.3 299.1 %all-gather.21.cloned.1.call-start = ((), (), s32[]{:S(2)}) async-start(), calls=%async_computation.9 | async-start | bytes 12255232 | tf_op jit(solution)/shard_map/all_gather | solution.py:72
  235.1 481.3 %all-gather.23.cloned.1.call-start = ((), (), s32[]{:S(2)}) async-start(), calls=%async_computation.10 | async-start | bytes 12255232 | tf_op jit(solution)/shard_map/all_gather | solution.py:76
  235.8 511.3 %reduce-scatter.5.cloned.1.call-start = ((), (), s32[]{:S(2)}) async-start(), calls=%async_computation.11 | async-start | bytes 3145728 | tf_op jit(solution)/shard_map/reduce_scatter | solution.py:79
  245.6 470.8 %copy-start.9 = (bf16[512,2048]{1,0:T(8,128)(2,1)S(1)}, bf16[512,2048]{1,0:T(8,128)(2,1)}, u32[]{:S(2)}) copy-start(bf16[512,2048]{1,0:T(8,128)(2,1)} %all-gather.17.cloned.1.call-done) | copy-start | bytes 6291460
  739.1 8.0 %copy-start = (bf16[512,1024]{1,0:T(8,128)(2,1)S(1)}, bf16[512,1024]{1,0:T(8,128)(2,1)}, u32[]{:S(2)}) copy-start(bf16[512,1024]{1,0:T(8,128)(2,1)} %multiply_convert_fusion.2) | copy-start | bytes 3145732
  739.1 12.4 %copy-start.6 = (f32[1024]{0:T(1024)S(1)}, f32[1024]{0:T(1024)}, u32[]{:S(2)}) copy-start(f32[1024]{0:T(1024)} %param.23) | copy-start | bytes 12292
  747.1 4.4 copy-start.3
Sparse Core Ops, SparseCore 0:
  8.9 13.2 all-gather.8
  25.0 61.5 all-gather.12
  89.3 59.1 all-gather.10
  151.1 61.7 all-gather.14
  219.8 7.7 reduce-scatter.2
  233.7 11.8 all-gather.16
  248.3 142.5 all-gather.18
  393.7 139.6 all-gather.20
  536.1 180.2 all-gather.22
  739.3 7.7 reduce-scatter.4
where the time goes:
time: 760 us
  waiting for transfers between devices  684 us (90%)
  matrix products  46.3 us (6%)
  between operations  13.6 us (2%)
    all_gather x1, waiting for transfers between devices, on_device(): lax.all_gather(down_weight, 'fs', axis=1, tiled=True)  183 us
    all_gather x1, waiting for transfers between devices, on_device(): gate = add_first(lax.all_gather(gate_weight, 'fs', axis=0, tiled=True))  145 us
    all_gather x1, waiting for transfers between devices, on_device(): upper = add_first(lax.all_gather(up_weight, 'fs', axis=0, tiled=True))  130 us
    all_gather x1, waiting for transfers between devices, on_device(): pre_v = add_one(lax.all_gather(v_weight, 'fs', axis=0, tiled=True))  64.4 us
    all_gather x1, waiting for transfers between devices, on_device(): lax.all_gather(out_weight, 'fs', axis=1, tiled=True)  64.3 us
    all_gather x1, waiting for transfers between devices, on_device(): pre_u = add_one(lax.all_gather(u_weight, 'fs', axis=0, tiled=True))  54.1 us
    dot_general x1, matrix products, on_device(): jnp.dot(hidden, lax.all_gather(down_weight, 'fs', axis=1, tiled=True), pr...  22.8 us
    dot_general x2, matrix products, add_rows(): return jnp.dot(left, piece, preferred_element_type=jnp.float32)  16.3 us
  transfers between devices with their start and end apart: 10, of which 10 were waited for; matrix products, arithmetic and copies ran while one was open for 2% of the time, Pallas kernels for 0%

commit v1 on v0

--- a/solution.py
+++ b/solution.py
@@ -5,6 +5,18 @@
 
 EPS = 1e-05
 ALPHA = 2.0**0.25
+
+
+def gather_by_bits(x, axis, dim):
+    ways, here, lap = (lax.axis_size(axis), lax.axis_index(axis), x.shape[dim])
+    line, have = (x, 1)
+    while have < ways:
+        line = jnp.concatenate(
+            [line, lax.ppermute(line, axis, [(d, (d - have) % ways) for d in range(ways)])],
+            axis=dim,
+        )
+        have = 2 * have
+    return jnp.roll(line, here * lap, axis=dim)
 
 
 def add_rows(left, piece):
@@ -39,7 +51,7 @@
     def add_one(piece):
         return add_rows(whole, piece)
 
-    pre_u = add_one(lax.all_gather(u_weight, "fs", axis=0, tiled=True))
+    pre_u = add_one(gather_by_bits(u_weight, "fs", 0))
     pre_v = add_one(lax.all_gather(v_weight, "fs", axis=0, tiled=True))
     gated = jax.nn.gelu(pre_u)
     valued = jax.nn.gelu(pre_v)

time: 760 us -> 733 us (0.964)
  waiting for transfers between devices: 684 us -> 638 us
  starting transfers between devices: 0.53 us -> 9.59 us
  local copies, waits for them, and re-layouts: 0.57 us -> 8.75 us
    ppermute x0 -> x4, waiting for transfers between devices: none -> 70.6 us  [gather_by_bits(): lax.ppermute(line, axis, [(d, (d - have) % ways) for d in range(ways)])]
    all_gather x1 -> x0, waiting for transfers between devices: 54.1 us -> none  [on_device(): pre_u = add_one(lax.all_gather(u_weight, 'fs', axis=0, tiled=True))]
    all_gather x1, waiting for transfers between devices: 64.4 us -> 24.3 us  [on_device(): pre_v = add_one(lax.all_gather(v_weight, 'fs', axis=0, tiled=True))]
    all_gather x1, waiting for transfers between devices: 12.8 us -> 0.01 us  [on_device(): whole = lax.all_gather(tokens, 'tp', axis=1, tiled=True)]
    ppermute x0 -> x4, starting transfers between devices: none -> 9.09 us  [gather_by_bits(): lax.ppermute(line, axis, [(d, (d - have) % ways) for d in range(ways)])]
    all_gather x1, waiting for transfers between devices: 64.3 us -> 56.4 us  [on_device(): lax.all_gather(out_weight, 'fs', axis=1, tiled=True)]
  transfers between devices with their start and end apart: 10 -> 13, of which waited for: 10 -> 12; matrix products, arithmetic and copies ran while one was open for 2% -> 4% of each run, Pallas kernels for 0% -> 0%
where the time goes in v1:
time: 733 us
  waiting for transfers between devices  638 us (87%)
  matrix products  46.3 us (6%)
  between operations  13.3 us (2%)
  starting transfers between devices  9.59 us (1%)
  other arithmetic  9.26 us (1%)
  local copies, waits for them, and re-layouts  8.75 us (1%)
  blocking collectives  7.54 us (1%)
    all_gather x1, waiting for transfers between devices, on_device(): lax.all_gather(down_weight, 'fs', axis=1, tiled=True)  183 us
    all_gather x1, waiting for transfers between devices, on_device(): gate = add_first(lax.all_gather(gate_weight, 'fs', axis=0, tiled=True))  145 us
    all_gather x1, waiting for transfers between devices, on_device(): upper = add_first(lax.all_gather(up_weight, 'fs', axis=0, tiled=True))  130 us
    ppermute x4, waiting for transfers between devices, gather_by_bits(): lax.ppermute(line, axis, [(d, (d - have) % ways) for d in range(ways)])  70.6 us
    all_gather x1, waiting for transfers between devices, on_device(): lax.all_gather(out_weight, 'fs', axis=1, tiled=True)  56.4 us
    all_gather x1, waiting for transfers between devices, on_device(): pre_v = add_one(lax.all_gather(v_weight, 'fs', axis=0, tiled=True))  24.3 us
    dot_general x1, matrix products, on_device(): jnp.dot(hidden, lax.all_gather(down_weight, 'fs', axis=1, tiled=True), pr...  22.8 us
    dot_general x2, matrix products, add_rows(): return jnp.dot(left, piece, preferred_element_type=jnp.float32)  16.3 us
  transfers between devices with their start and end apart: 13, of which 12 were waited for; matrix products, arithmetic and copies ran while one was open for 4% of the time, Pallas kernels for 0%

profile of v1, /device:TPU:0, one launch (start us, length us, event | category | flops | bytes accessed | tf_op | source)
XLA Modules:
  0.0 733.2 jit_solution(17388380341607111629)
XLA Ops:
  8.1 7.0 collective-permute-start
  15.1 3.1 collective-permute-done
  20.6 5.7 collective-permute-done.1
  27.8 12.4 %collective-permute-done.2 = bf16[512,512]{1,0:T(8,128)(2,1)S(1)} collective-permute-done((bf16[512,512]{1,0:T(8,128)(2,1)S(1)}, bf16[512,512]{1,0:T(8,128)(2,1)S(1)}, u32[]{:S(2)}, u32[]{:S(2)}) %collective-permute-start.2) | collective-permute-done | bytes 524320 | tf_op jit(solution)/shard_map/ppermute | solution.py:15
  43.3 49.4 %collective-permute-done.3 = bf16[1024,512]{1,0:T(8,128)(2,1)S(1)} collective-permute-done((bf16[1024,512]{1,0:T(8,128)(2,1)S(1)}, bf16[1024,512]{1,0:T(8,128)(2,1)S(1)}, u32[]{:S(2)}, u32[]{:S(2)}) %collective-permute-start.3) | collective-permute-done | bytes 1048608 | tf_op jit(solution)/shard_map/ppermute | solution.py:15
  97.7 24.3 %all-gather.10.cloned.1.call-done = bf16[2048,512]{1,0:T(8,128)(2,1)} async-done(((bf16[128,512]{1,0:T(8,128)(2,1)}), bf16[2048,512]{1,0:T(8,128)(2,1)}) %all-gather.10.cloned.1.call-update) | async-done | bytes 2097168 | tf_op jit(solution)/shard_map/all_gather | solution.py:55
  122.1 3.8 fusion.49
  125.9 2.6 all-reduce.2
  130.1 56.4 %all-gather.12.cloned.1.call-done = bf16[512,2048]{1,0:T(8,128)(2,1)} async-done(((bf16[512,128]{1,0:T(8,128)(2,1)}), bf16[512,2048]{1,0:T(8,128)(2,1)}) %all-gather.12.cloned.1.call-update) | async-done | bytes 2097168 | tf_op jit(solution)/shard_map/all_gather | solution.py:71
  186.5 6.9 convolution_convert_fusion.1
  193.5 7.9 %reduce-scatter.3.cloned.1.call-done = bf16[512,1024]{1,0:T(8,128)(2,1)} async-done(((bf16[512,2048]{1,0:T(8,128)(2,1)}), bf16[512,1024]{1,0:T(8,128)(2,1)}) %reduce-scatter.3.cloned.1.call-update) | async-done | bytes 1048592 | tf_op jit(solution)/shard_map/reduce_scatter | solution.py:74
  201.4 1.9 fusion.2
  203.3 2.5 all-reduce.1
  205.8 1.5 multiply_convert_fusion.2
  209.7 9.7 %all-gather.14.cloned.1.call-done = bf16[512,2048]{1,0:T(8,128)(2,1)} async-done(((bf16[512,1024]{1,0:T(8,128)(2,1)}), bf16[512,2048]{1,0:T(8,128)(2,1)}) %all-gather.14.cloned.1.call-update) | async-done | bytes 2097168 | tf_op jit(solution)/shard_map/all_gather | solution.py:78
  219.4 145.2 %all-gather.16.cloned.1.call-done = bf16[2048,2816]{1,0:T(8,128)(2,1)} async-done(((bf16[128,2816]{1,0:T(8,128)(2,1)}), bf16[2048,2816]{1,0:T(8,128)(2,1)}) %all-gather.16.cloned.1.call-update) | async-done | bytes 11534352 | tf_op jit(solution)/shard_map/all_gather | solution.py:83
  364.6 12.5 %fusion.50 = f32[512,2816]{1,0:T(8,128)} fusion(bf16[512,2048]{1,0:T(8,128)(2,1)} %all-gather.14.cloned.1.call-done, bf16[2048,2816]{1,0:T(8,128)(2,1)} %all-gather.16.cloned.1.call-done), kind=kOutput, calls=%fused_computation.73 | convolution fusion | flops 5905580032 | bytes 19398656 | tf_op jit(solution)/shard_map/dot_general | solution.py:23
  377.1 130.0 %all-gather.18.cloned.1.call-done = bf16[2048,2816]{1,0:T(8,128)(2,1)} async-done(((bf16[128,2816]{1,0:T(8,128)(2,1)}), bf16[2048,2816]{1,0:T(8,128)(2,1)}) %all-gather.18.cloned.1.call-update) | async-done | bytes 11534352 | tf_op jit(solution)/shard_map/all_gather | solution.py:84
  507.0 183.0 %all-gather.20.cloned.1.call-done = bf16[2816,2048]{1,0:T(8,128)(2,1)} async-done(((bf16[2816,128]{1,0:T(8,128)(2,1)}), bf16[2816,2048]{1,0:T(8,128)(2,1)}) %all-gather.20.cloned.1.call-update) | async-done | bytes 11534352 | tf_op jit(solution)/shard_map/all_gather | solution.py:88
  690.0 22.8 %convolution_convert_fusion = bf16[512,2048]{1,0:T(8,128)(2,1)} fusion(bf16[2816,2048]{1,0:T(8,128)(2,1)} %all-gather.20.cloned.1.call-done, f32[512,2816]{1,0:T(8,128)} %fusion.50, bf16[512,2048]{1,0:T(8,128)(2,1)S(1)} %copy-done.10, bf16[2048,2816]{1,0:T(8,128)(2,1)} %all-gather.18.cloned.1.call-done), kind=kOutput, calls=%fused_computation.1 | convolution fusion | flops 11820859392 | bytes 33030144 | tf_op jit(solution)/shard_map/dot_general | solution.py:86
  712.8 8.0 %reduce-scatter.5.cloned.1.call-done = bf16[512,1024]{1,0:T(8,128)(2,1)} async-done(((bf16[512,2048]{1,0:T(8,128)(2,1)}), bf16[512,1024]{1,0:T(8,128)(2,1)}) %reduce-scatter.5.cloned.1.call-update) | async-done | bytes 1048592 | tf_op jit(solution)/shard_map/reduce_scatter | solution.py:91
  720.8 1.9 fusion.3
  722.7 2.5 all-reduce
  725.2 1.5 multiply_convert_fusion.1
  (65 shorter events, 17.4 us)
Async XLA Ops:
  6.5 33.7 %copy-start.4 = (bf16[128,512]{1,0:T(8,128)(2,1)S(1)}, bf16[128,512]{1,0:T(8,128)(2,1)}, u32[]{:S(2)}) copy-start(bf16[128,512]{1,0:T(8,128)(2,1)} %param.13) | copy-start | bytes 393220
  6.5 91.2 %all-gather.8.cloned.1.call-start = ((), (), s32[]{:S(2)}) async-start(), calls=%async_computation.2 | async-start | bytes 3145728 | tf_op jit(solution)/shard_map/all_gather | solution.py:47
  7.3 114.8 %all-gather.10.cloned.1.call-start = ((), (), s32[]{:S(2)}) async-start(), calls=%async_computation.3 | async-start | bytes 2228224 | tf_op jit(solution)/shard_map/all_gather | solution.py:55
  8.0 178.5 %all-gather.12.cloned.1.call-start = ((), (), s32[]{:S(2)}) async-start(), calls=%async_computation.4 | async-start | bytes 2228224 | tf_op jit(solution)/shard_map/all_gather | solution.py:71
  8.1 10.1 %collective-permute-start = (bf16[128,512]{1,0:T(8,128)(2,1)}, bf16[128,512]{1,0:T(8,128)(2,1)S(1)}, u32[]{:S(2)}, u32[]{:S(2)}) collective-permute-start(bf16[128,512]{1,0:T(8,128)(2,1)} %param.13), channel_id=1, source_target_pairs={{0,30},{2,0},{4,2},{6,4},{8,6},{10,8},{12,10},{14,12},{16,14},{18,... | collective-permute-start | bytes 393224 | tf_op jit(solution)/shard_map/ppermute | solution.py:15
  19.1 7.2 collective-permute-start.1
  20.6 180.8 %reduce-scatter.3.cloned.1.call-start = ((), (), s32[]{:S(2)}) async-start(), calls=%async_computation.5 | async-start | bytes 3145728 | tf_op jit(solution)/shard_map/reduce_scatter | solution.py:74
  27.3 12.9 %collective-permute-start.2 = (bf16[512,512]{1,0:T(8,128)(2,1)S(1)}, bf16[512,512]{1,0:T(8,128)(2,1)S(1)}, u32[]{:S(2)}, u32[]{:S(2)}) collective-permute-start(bf16[512,512]{1,0:T(8,128)(2,1)S(1)} %pad_maximum_fusion.1), channel_id=1, source_target_pairs={{0,24},{2,26},{4,28},{6,30},{8,0},{10,2},{12,4},{14,6},{16,8},{18,... | collective-permute-start | bytes 1572872 | tf_op jit(solution)/shard_map/ppermute | solution.py:15
  40.3 52.4 %collective-permute-start.3 = (bf16[1024,512]{1,0:T(8,128)(2,1)S(1)}, bf16[1024,512]{1,0:T(8,128)(2,1)S(1)}, u32[]{:S(2)}, u32[]{:S(2)}) collective-permute-start(bf16[1024,512]{1,0:T(8,128)(2,1)S(1)} %pad_maximum_fusion), channel_id=1, source_target_pairs={{0,16},{2,18},{4,20},{6,22},{8,24},{10,26},{12,28},{14,30},{16,0},... | collective-permute-start | bytes 3145736 | tf_op jit(solution)/shard_map/ppermute | solution.py:15
  97.7 30.8 %copy-start.8 = (f32[512]{0:T(512)S(1)}, f32[512]{0:T(512)}, u32[]{:S(2)}) copy-start(f32[512]{0:T(512)} %param.15) | copy-start | bytes 6148
  125.9 3.2 copy-start.5
  125.9 3.2 copy-start.9
  193.5 8.0 %copy-start.1 = (bf16[512,1024]{1,0:T(8,128)(2,1)S(1)}, bf16[512,1024]{1,0:T(8,128)(2,1)}, u32[]{:S(2)}) copy-start(bf16[512,1024]{1,0:T(8,128)(2,1)} %param.12) | copy-start | bytes 3145732
  193.5 12.4 %copy-start.6 = (f32[1024]{0:T(1024)S(1)}, f32[1024]{0:T(1024)}, u32[]{:S(2)}) copy-start(f32[1024]{0:T(1024)} %param.19) | copy-start | bytes 12292
  193.5 25.9 %all-gather.14.cloned.1.call-start = ((), (), s32[]{:S(2)}) async-start(), calls=%async_computation.6 | async-start | bytes 3145728 | tf_op jit(solution)/shard_map/all_gather | solution.py:78
  201.4 4.4 copy-start.2
  207.4 157.2 %all-gather.16.cloned.1.call-start = ((), (), s32[]{:S(2)}) async-start(), calls=%async_computation.7 | async-start | bytes 12255232 | tf_op jit(solution)/shard_map/all_gather | solution.py:83
  207.9 299.1 %all-gather.18.cloned.1.call-start = ((), (), s32[]{:S(2)}) async-start(), calls=%async_computation.8 | async-start | bytes 12255232 | tf_op jit(solution)/shard_map/all_gather | solution.py:84
  208.7 481.3 %all-gather.20.cloned.1.call-start = ((), (), s32[]{:S(2)}) async-start(), calls=%async_computation.9 | async-start | bytes 12255232 | tf_op jit(solution)/shard_map/all_gather | solution.py:88
  209.4 511.3 %reduce-scatter.5.cloned.1.call-start = ((), (), s32[]{:S(2)}) async-start(), calls=%async_computation.10 | async-start | bytes 3145728 | tf_op jit(solution)/shard_map/reduce_scatter | solution.py:91
  219.4 470.6 %copy-start.10 = (bf16[512,2048]{1,0:T(8,128)(2,1)S(1)}, bf16[512,2048]{1,0:T(8,128)(2,1)}, u32[]{:S(2)}) copy-start(bf16[512,2048]{1,0:T(8,128)(2,1)} %all-gather.14.cloned.1.call-done) | copy-start | bytes 6291460
  712.8 8.0 %copy-start = (bf16[512,1024]{1,0:T(8,128)(2,1)S(1)}, bf16[512,1024]{1,0:T(8,128)(2,1)}, u32[]{:S(2)}) copy-start(bf16[512,1024]{1,0:T(8,128)(2,1)} %multiply_convert_fusion.2) | copy-start | bytes 3145732
  712.8 12.4 %copy-start.7 = (f32[1024]{0:T(1024)S(1)}, f32[1024]{0:T(1024)}, u32[]{:S(2)}) copy-start(f32[1024]{0:T(1024)} %param.23) | copy-start | bytes 12292
  720.8 4.4 copy-start.3
Sparse Core Ops, SparseCore 0:
  8.9 13.2 all-gather.7
  25.0 97.0 all-gather.9
  124.8 61.7 all-gather.11
  193.6 7.7 reduce-scatter.2
  207.5 11.8 all-gather.13
  222.0 142.5 all-gather.15
  367.4 139.6 all-gather.17
  509.7 180.2 all-gather.19
  712.9 7.7 reduce-scatter.4
